TPU v7x, 32 devices: a whole 2x2x4 slice. The times are simulated.
32 devices in a mesh: rep: 2 (over x), fs: 8 (over z, y), tp: 2 (over core).
Axes of the slice: x: 2, y: 2, z: 4, core: 2. Of those that a mesh axis runs over, the one named last changes fastest.
Arguments:
- tokens: bfloat16 [4096, 2048], P(('rep', 'fs', 'tp')), may hold values from -6 to 6
- mix_gain: float32 [2048], replicated, may hold values from 0.1 to 1.9
- conv_in_weight: bfloat16 [2048, 1024], P('fs', 'tp'), may hold values from -0.125 to 0.125
- gate_outer_weight: bfloat16 [2048, 1024], P('fs', 'tp'), may hold values from -0.125 to 0.125
- gate_inner_weight: bfloat16 [2048, 1024], P('fs', 'tp'), may hold values from -0.125 to 0.125
- conv_taps: float32 [3, 1024], P(None, 'tp'), may hold values from -3.5 to 3.5
- out_weight: bfloat16 [1024, 2048], P('tp', 'fs'), may hold values from -0.1875 to 0.1875
- ff_gain: float32 [2048], replicated, may hold values from 0.1 to 1.9
- up_weight: bfloat16 [2048, 8192], P('fs', 'tp'), may hold values from -0.125 to 0.125
- down_weight: bfloat16 [8192, 2048], P('tp', 'fs'), may hold values from -0.0625 to 0.0625
Outputs:
- layer_out: bfloat16 [4096, 2048], P(('rep', 'fs', 'tp'))
All inputs are finite; a program needn't handle non-finite values.
Results may differ from a plain program's by a relative error of at most 0.023.
Values may be sent and summed in bfloat16 or wider, within the bound.
A program may use at most 128 MiB of HBM per device.

v0:
```python
import jax
import jax.numpy as jnp
from jax import lax
from jax.sharding import PartitionSpec as P

eps = 1e-06


def rms_scale(values, gain):
    widened = values.astype(jnp.float32)
    inverse = lax.rsqrt(jnp.mean(widened * widened, axis=-1, keepdims=True) + eps)
    return (widened * inverse * gain).astype(jnp.bfloat16)


def on_device(
    tokens,
    mix_gain,
    conv_in_weight,
    gate_outer_weight,
    gate_inner_weight,
    conv_taps,
    out_weight,
    ff_gain,
    up_weight,
    down_weight,
):
    normed = rms_scale(tokens, mix_gain)
    gathered = lax.all_gather(normed, "tp", axis=0, tiled=True)
    seq_rows = gathered.shape[0]
    segment = (
        lax.all_gather(conv_in_weight, "fs", axis=0, tiled=True),
        lax.all_gather(gate_outer_weight, "fs", axis=0, tiled=True),
        lax.all_gather(gate_inner_weight, "fs", axis=0, tiled=True),
    )
    conv_input, gate_outer, gate_inner = tuple(
        (jnp.dot(gathered, weight, preferred_element_type=jnp.float32) for weight in segment)
    )
    conv_input = conv_input.astype(jnp.bfloat16)
    gate_outer = gate_outer.astype(jnp.bfloat16)
    gate_inner = gate_inner.astype(jnp.bfloat16)
    gated = gate_inner.astype(jnp.float32) * conv_input.astype(jnp.float32)
    padded = jnp.pad(gated, ((2, 0), (0, 0)))
    convolved = (
        conv_taps[0] * padded[0:seq_rows]
        + conv_taps[1] * padded[1 : seq_rows + 1]
        + conv_taps[2] * padded[2 : seq_rows + 2]
    )
    mixed = (gate_outer.astype(jnp.float32) * convolved).astype(jnp.bfloat16)
    out_full = lax.all_gather(out_weight, "fs", axis=1, tiled=True)
    lefts = mixed
    mix_total = lax.psum_scatter(
        jnp.dot(lefts, out_full, preferred_element_type=jnp.float32).astype(jnp.bfloat16),
        "tp",
        scatter_dimension=0,
        tiled=True,
    ).astype(jnp.float32)
    resid = (tokens.astype(jnp.float32) + mix_total).astype(jnp.bfloat16)
    normed_ff = rms_scale(resid, ff_gain)
    ff_gathered = lax.all_gather(normed_ff, "tp", axis=0, tiled=True)
    up_full = lax.all_gather(up_weight, "fs", axis=0, tiled=True)
    preact = jnp.dot(ff_gathered, up_full, preferred_element_type=jnp.float32)
    hidden = jnp.square(jax.nn.relu(preact)).astype(jnp.bfloat16)
    down_full = lax.all_gather(down_weight, "fs", axis=1, tiled=True)
    lefts = hidden
    ff_total = lax.psum_scatter(
        jnp.dot(lefts, down_full, preferred_element_type=jnp.float32).astype(jnp.bfloat16),
        "tp",
        scatter_dimension=0,
        tiled=True,
    ).astype(jnp.float32)
    return (resid.astype(jnp.float32) + ff_total).astype(jnp.bfloat16)


def solution(mesh):
    in_specs = (
        P(("rep", "fs", "tp"), None),
        P(),
        P("fs", "tp"),
        P("fs", "tp"),
        P("fs", "tp"),
        P(None, "tp"),
        P("tp", "fs"),
        P(),
        P("fs", "tp"),
        P("tp", "fs"),
    )
    out_specs = P(("rep", "fs", "tp"), None)
    return jax.shard_map(
        on_device, mesh=mesh, in_specs=in_specs, out_specs=out_specs, check_vma=False
    )
```

profile of v0, /device:TPU:0, one launch (start us, length us, event | category | flops | bytes accessed | tf_op | source)
XLA Modules:
  0.0 740.0 jit_solution(13610082769893983982)
XLA Ops:
  6.5 0.0 copy-start.4
  6.5 0.0 all-gather.9.cloned.1.call-start
  6.5 1.2 fusion.8
  7.8 2.0 fusion.10
  9.8 0.0 all-gather.9.cloned.1.call-update
  9.8 0.0 all-gather.15.cloned.1.call-start
  9.9 0.7 all-gather.15.cloned.1.call-update
  10.6 0.0 all-gather.13.cloned.1.call-start
  10.6 0.7 all-gather.13.cloned.1.call-update
  11.3 0.0 all-gather.11.cloned.1.call-start
  11.4 0.5 all-gather.11.cloned.1.call-update
  11.9 0.0 all-gather.17.cloned.1.call-start
  12.0 0.5 all-gather.17.cloned.1.call-update
  12.5 0.0 reduce-scatter.3.cloned.1.call-start
  12.5 0.0 copy-done.4
  12.6 9.2 %all-gather.9.cloned.1.call-done = bf16[256,2048]{1,0:T(8,128)(2,1)} async-done(((bf16[128,2048]{1,0:T(8,128)(2,1)}), bf16[256,2048]{1,0:T(8,128)(2,1)}) %all-gather.9.cloned.1.call-update) | async-done | bytes 1048592 | tf_op jit(solution)/shard_map/all_gather | solution.py:28
  21.7 0.0 copy-start.2
  21.7 52.4 %all-gather.15.cloned.1.call-done = bf16[2048,512]{1,0:T(8,128)(2,1)} async-done(((bf16[256,512]{1,0:T(8,128)(2,1)}), bf16[2048,512]{1,0:T(8,128)(2,1)}) %all-gather.15.cloned.1.call-update) | async-done | bytes 2097168 | tf_op jit(solution)/shard_map/all_gather | solution.py:31
  74.2 2.6 fusion.7
  76.8 47.2 %all-gather.13.cloned.1.call-done = bf16[2048,512]{1,0:T(8,128)(2,1)} async-done(((bf16[256,512]{1,0:T(8,128)(2,1)}), bf16[2048,512]{1,0:T(8,128)(2,1)}) %all-gather.13.cloned.1.call-update) | async-done | bytes 2097168 | tf_op jit(solution)/shard_map/all_gather | solution.py:33
  123.9 0.0 copy-done.2
  124.0 2.3 fusion.6
  126.3 47.3 %all-gather.11.cloned.1.call-done = bf16[2048,512]{1,0:T(8,128)(2,1)} async-done(((bf16[256,512]{1,0:T(8,128)(2,1)}), bf16[2048,512]{1,0:T(8,128)(2,1)}) %all-gather.11.cloned.1.call-update) | async-done | bytes 2097168 | tf_op jit(solution)/shard_map/all_gather | solution.py:32
  173.6 50.8 %all-gather.17.cloned.1.call-done = bf16[512,2048]{1,0:T(8,128)(2,1)} async-done(((bf16[512,256]{1,0:T(8,128)(2,1)}), bf16[512,2048]{1,0:T(8,128)(2,1)}) %all-gather.17.cloned.1.call-update) | async-done | bytes 2097168 | tf_op jit(solution)/shard_map/all_gather | solution.py:49
  224.4 0.0 copy-start
  224.4 4.7 convolution_convert_fusion.1
  229.1 0.0 copy-start.3
  229.1 0.0 reduce-scatter.3.cloned.1.call-update
  229.1 0.0 all-gather.19.cloned.1.call-start
  229.2 6.7 reduce-scatter.3.cloned.1.call-done
  235.8 0.0 copy-done
  235.9 1.3 fusion.12
  237.2 0.0 copy-done.3
  237.2 2.0 fusion.14
  239.2 0.0 all-gather.19.cloned.1.call-update
  239.2 0.0 all-gather.21.cloned.1.call-start
  239.3 0.7 all-gather.21.cloned.1.call-update
  240.0 0.0 all-gather.23.cloned.1.call-start
  240.0 0.7 all-gather.23.cloned.1.call-update
  240.7 0.0 copy-start.1
  240.7 0.0 reduce-scatter.5.cloned.1.call-start
  240.8 8.9 %all-gather.19.cloned.1.call-done = bf16[256,2048]{1,0:T(8,128)(2,1)} async-done(((bf16[128,2048]{1,0:T(8,128)(2,1)}), bf16[256,2048]{1,0:T(8,128)(2,1)}) %all-gather.19.cloned.1.call-update) | async-done | bytes 1048592 | tf_op jit(solution)/shard_map/all_gather | solution.py:59
  249.6 230.6 %all-gather.21.cloned.1.call-done = bf16[2048,4096]{1,0:T(8,128)(2,1)} async-done(((bf16[256,4096]{1,0:T(8,128)(2,1)}), bf16[2048,4096]{1,0:T(8,128)(2,1)}) %all-gather.21.cloned.1.call-update) | async-done | bytes 16777232 | tf_op jit(solution)/shard_map/all_gather | solution.py:60
  480.2 227.6 %all-gather.23.cloned.1.call-done = bf16[4096,2048]{1,0:T(8,128)(2,1)} async-done(((bf16[4096,256]{1,0:T(8,128)(2,1)}), bf16[4096,2048]{1,0:T(8,128)(2,1)}) %all-gather.23.cloned.1.call-update) | async-done | bytes 16777232 | tf_op jit(solution)/shard_map/all_gather | solution.py:63
  707.8 16.5 %convolution_convert_fusion = bf16[256,2048]{1,0:T(8,128)(2,1)} fusion(bf16[4096,2048]{1,0:T(8,128)(2,1)} %all-gather.23.cloned.1.call-done, bf16[256,2048]{1,0:T(8,128)(2,1)} %all-gather.19.cloned.1.call-done, bf16[2048,4096]{1,0:T(8,128)(2,1)} %all-gather.21.cloned.1.call-done), kind=kOutput, calls=%fused_computation.3 | convolution fusion | flops 8593604608 | bytes 35651584 | tf_op jit(solution)/shard_map/dot_general | solution.py:66
  724.3 0.0 reduce-scatter.5.cloned.1.call-update
  724.4 6.7 reduce-scatter.5.cloned.1.call-done
  731.1 0.0 copy-done.1
  731.1 2.1 fusion.15
  (3 shorter events, 0.0 us)
Async XLA Ops:
  6.5 6.0 copy-start.4
  6.5 15.2 %all-gather.9.cloned.1.call-start = ((), (), s32[]{:S(2)}) async-start(), calls=%async_computation.2 | async-start | bytes 1572864 | tf_op jit(solution)/shard_map/all_gather | solution.py:28
  9.8 64.3 %all-gather.15.cloned.1.call-start = ((), (), s32[]{:S(2)}) async-start(), calls=%async_computation.5 | async-start | bytes 2359296 | tf_op jit(solution)/shard_map/all_gather | solution.py:31
  10.6 113.4 %all-gather.13.cloned.1.call-start = ((), (), s32[]{:S(2)}) async-start(), calls=%async_computation.4 | async-start | bytes 2359296 | tf_op jit(solution)/shard_map/all_gather | solution.py:33
  11.3 162.3 %all-gather.11.cloned.1.call-start = ((), (), s32[]{:S(2)}) async-start(), calls=%async_computation.3 | async-start | bytes 2359296 | tf_op jit(solution)/shard_map/all_gather | solution.py:32
  11.9 212.5 %all-gather.17.cloned.1.call-start = ((), (), s32[]{:S(2)}) async-start(), calls=%async_computation.6 | async-start | bytes 2359296 | tf_op jit(solution)/shard_map/all_gather | solution.py:49
  12.5 223.4 %reduce-scatter.3.cloned.1.call-start = ((), (), s32[]{:S(2)}) async-start(), calls=%async_computation.7 | async-start | bytes 1572864 | tf_op jit(solution)/shard_map/reduce_scatter | solution.py:51
  21.7 102.2 %copy-start.2 = (bf16[256,2048]{1,0:T(8,128)(2,1)S(1)}, bf16[256,2048]{1,0:T(8,128)(2,1)}, u32[]{:S(2)}) copy-start(bf16[256,2048]{1,0:T(8,128)(2,1)} %all-gather.9.cloned.1.call-done) | copy-start | bytes 3145732
  224.4 11.5 %copy-start = (bf16[128,2048]{1,0:T(8,128)(2,1)S(1)}, bf16[128,2048]{1,0:T(8,128)(2,1)}, u32[]{:S(2)}) copy-start(bf16[128,2048]{1,0:T(8,128)(2,1)} %param.10) | copy-start | bytes 1572868
  229.1 8.1 %copy-start.3 = (f32[2048]{0:T(1024)S(1)}, f32[2048]{0:T(1024)}, u32[]{:S(2)}) copy-start(f32[2048]{0:T(1024)} %param.17) | copy-start | bytes 24580
  229.1 20.5 %all-gather.19.cloned.1.call-start = ((), (), s32[]{:S(2)}) async-start(), calls=%async_computation.8 | async-start | bytes 1572864 | tf_op jit(solution)/shard_map/all_gather | solution.py:59
  239.2 241.0 %all-gather.21.cloned.1.call-start = ((), (), s32[]{:S(2)}) async-start(), calls=%async_computation.9 | async-start | bytes 18874368 | tf_op jit(solution)/shard_map/all_gather | solution.py:60
  240.0 467.8 %all-gather.23.cloned.1.call-start = ((), (), s32[]{:S(2)}) async-start(), calls=%async_computation.10 | async-start | bytes 18874368 | tf_op jit(solution)/shard_map/all_gather | solution.py:63
  240.7 490.4 %copy-start.1 = (bf16[128,2048]{1,0:T(8,128)(2,1)S(1)}, bf16[128,2048]{1,0:T(8,128)(2,1)}, u32[]{:S(2)}) copy-start(bf16[128,2048]{1,0:T(8,128)(2,1)} %reduce-scatter.3.cloned.1.call-done) | copy-start | bytes 1572868
  240.7 490.4 %reduce-scatter.5.cloned.1.call-start = ((), (), s32[]{:S(2)}) async-start(), calls=%async_computation.11 | async-start | bytes 1572864 | tf_op jit(solution)/shard_map/reduce_scatter | solution.py:65
Sparse Core Ops, SparseCore 0:
  10.0 11.7 all-gather.8
  23.9 50.2 all-gather.14
  76.3 47.6 all-gather.12
  125.9 47.6 all-gather.10
  175.5 48.8 all-gather.16
  229.2 6.5 reduce-scatter.2
  239.3 10.2 all-gather.18
  251.7 228.4 all-gather.20
  482.3 225.4 all-gather.22
  724.5 6.5 reduce-scatter.4
where the time goes:
time: 740 us
  waiting for transfers between devices  691 us (93%)
  matrix products  26.2 us (4%)
  between operations  13.6 us (2%)
  other arithmetic  8.69 us (1%)
    all_gather x1, waiting for transfers between devices, on_device(): up_full = lax.all_gather(up_weight, 'fs', axis=0, tiled=True)  231 us
    all_gather x1, waiting for transfers between devices, on_device(): down_full = lax.all_gather(down_weight, 'fs', axis=1, tiled=True)  228 us
    all_gather x1, waiting for transfers between devices, on_device(): lax.all_gather(conv_in_weight, 'fs', axis=0, tiled=True)  52.4 us
    all_gather x1, waiting for transfers between devices, on_device(): out_full = lax.all_gather(out_weight, 'fs', axis=1, tiled=True)  50.8 us
    all_gather x1, waiting for transfers between devices, on_device(): lax.all_gather(gate_outer_weight, 'fs', axis=0, tiled=True)  47.3 us
    all_gather x1, waiting for transfers between devices, on_device(): lax.all_gather(gate_inner_weight, 'fs', axis=0, tiled=True)  47.2 us
    dot_general x1, matrix products, on_device(): jnp.dot(lefts, down_full, preferred_element_type=jnp.float32)  16.5 us
  transfers between devices with their start and end apart: 10, of which 10 were waited for; matrix products, arithmetic and copies ran while one was open for 1% of the time, Pallas kernels for 0%

commit v1 on v0

--- a/solution.py
+++ b/solution.py
@@ -46,7 +46,12 @@
         + conv_taps[2] * padded[2 : seq_rows + 2]
     )
     mixed = (gate_outer.astype(jnp.float32) * convolved).astype(jnp.bfloat16)
-    out_full = lax.all_gather(out_weight, "fs", axis=1, tiled=True)
+    ring = [out_weight]
+    for hop in range(7):
+        ring.append(lax.ppermute(ring[-1], "fs", [(dev, (dev + 1) % 8) for dev in range(8)]))
+    out_full = jnp.roll(
+        jnp.concatenate(ring[::-1], axis=1), (lax.axis_index("fs") + 1) * ring[0].shape[1], axis=1
+    )
     lefts = mixed
     mix_total = lax.psum_scatter(
         jnp.dot(lefts, out_full, preferred_element_type=jnp.float32).astype(jnp.bfloat16),

time: 740 us -> 704 us (0.951)
  waiting for transfers between devices: 691 us -> 639 us
  local copies, waits for them, and re-layouts: 0.03 us -> 12.8 us
    ppermute x0 -> x7, waiting for transfers between devices: none -> 84.9 us  [on_device(): lax.ppermute(ring[-1], 'fs', [(dev, (dev + 1) % 8) for dev in range(8)])]
    all_gather x1, waiting for transfers between devices: 52.4 us -> 0.01 us  [on_device(): lax.all_gather(conv_in_weight, 'fs', axis=0, tiled=True)]
    all_gather x1 -> x0, waiting for transfers between devices: 50.8 us -> none  [on_device(): out_full = lax.all_gather(out_weight, 'fs', axis=1, tiled=True)]
    all_gather x1, waiting for transfers between devices: 47.2 us -> 23.5 us  [on_device(): lax.all_gather(gate_inner_weight, 'fs', axis=0, tiled=True)]
    unnamed x10 -> x25, local copies, waits for them, and re-layouts: 0.02 us -> 11.2 us
    all_gather x1, waiting for transfers between devices: 9.18 us -> 0.01 us  [on_device(): gathered = lax.all_gather(normed, 'tp', axis=0, tiled=True)]
  transfers between devices with their start and end apart: 10 -> 16, of which waited for: 10 -> 14; matrix products, arithmetic and copies ran while one was open for 1% -> 3% of each run, Pallas kernels for 0% -> 0%
where the time goes in v1:
time: 704 us
  waiting for transfers between devices  639 us (91%)
  matrix products  26.4 us (4%)
  between operations  13.3 us (2%)
  local copies, waits for them, and re-layouts  12.8 us (2%)
  other arithmetic  8.73 us (1%)
    all_gather x1, waiting for transfers between devices, on_device(): up_full = lax.all_gather(up_weight, 'fs', axis=0, tiled=True)  231 us
    all_gather x1, waiting for transfers between devices, on_device(): down_full = lax.all_gather(down_weight, 'fs', axis=1, tiled=True)  228 us
    ppermute x7, waiting for transfers between devices, on_device(): lax.ppermute(ring[-1], 'fs', [(dev, (dev + 1) % 8) for dev in range(8)])  84.9 us
    all_gather x1, waiting for transfers between devices, on_device(): lax.all_gather(gate_outer_weight, 'fs', axis=0, tiled=True)  47 us
    all_gather x1, waiting for transfers between devices, on_device(): lax.all_gather(gate_inner_weight, 'fs', axis=0, tiled=True)  23.5 us
    dot_general x1, matrix products, on_device(): jnp.dot(lefts, down_full, preferred_element_type=jnp.float32)  16.5 us
  transfers between devices with their start and end apart: 16, of which 14 were waited for; matrix products, arithmetic and copies ran while one was open for 3% of the time, Pallas kernels for 0%

profile of v1, /device:TPU:0, one launch (start us, length us, event | category | flops | bytes accessed | tf_op | source)
XLA Modules:
  0.0 703.7 jit_solution(15362884891319000877)
XLA Ops:
  6.5 1.3 fusion.9
  7.8 2.0 fusion.11
  9.8 0.0 all-gather.8.cloned.1.call-update
  9.9 0.0 all-gather.14.cloned.1.call-start
  9.9 0.7 all-gather.14.cloned.1.call-update
  10.6 0.0 all-gather.12.cloned.1.call-start
  10.7 0.7 all-gather.12.cloned.1.call-update
  11.4 0.0 all-gather.10.cloned.1.call-start
  11.4 3.0 collective-permute-start
  14.5 9.6 %collective-permute-done = bf16[512,256]{1,0:T(8,128)(2,1)S(1)} collective-permute-done((bf16[512,256]{1,0:T(8,128)(2,1)}, bf16[512,256]{1,0:T(8,128)(2,1)S(1)}, u32[]{:S(2)}, u32[]{:S(2)}) %collective-permute-start) | collective-permute-done | bytes 262176 | tf_op jit(solution)/shard_map/ppermute | solution.py:51
  24.0 0.0 collective-permute-start.1
  24.0 10.2 %collective-permute-done.1 = bf16[512,256]{1,0:T(8,128)(2,1)S(1)} collective-permute-done((bf16[512,256]{1,0:T(8,128)(2,1)S(1)}, bf16[512,256]{1,0:T(8,128)(2,1)S(1)}, u32[]{:S(2)}, u32[]{:S(2)}) %collective-permute-start.1) | collective-permute-done | bytes 262176 | tf_op jit(solution)/shard_map/ppermute | solution.py:51
  34.2 0.0 collective-permute-start.2
  34.2 0.0 all-gather.10.cloned.1.call-update
  34.2 0.0 reduce-scatter.3.cloned.1.call-start
  34.3 16.0 %collective-permute-done.2 = bf16[512,256]{1,0:T(8,128)(2,1)S(1)} collective-permute-done((bf16[512,256]{1,0:T(8,128)(2,1)S(1)}, bf16[512,256]{1,0:T(8,128)(2,1)S(1)}, u32[]{:S(2)}, u32[]{:S(2)}) %collective-permute-start.2) | collective-permute-done | bytes 262176 | tf_op jit(solution)/shard_map/ppermute | solution.py:51
  50.3 0.0 collective-permute-start.3
  50.3 9.1 %collective-permute-done.3 = bf16[512,256]{1,0:T(8,128)(2,1)S(1)} collective-permute-done((bf16[512,256]{1,0:T(8,128)(2,1)S(1)}, bf16[512,256]{1,0:T(8,128)(2,1)S(1)}, u32[]{:S(2)}, u32[]{:S(2)}) %collective-permute-start.3) | collective-permute-done | bytes 262176 | tf_op jit(solution)/shard_map/ppermute | solution.py:51
  59.3 0.0 collective-permute-start.4
  59.3 16.6 %collective-permute-done.4 = bf16[512,256]{1,0:T(8,128)(2,1)S(1)} collective-permute-done((bf16[512,256]{1,0:T(8,128)(2,1)S(1)}, bf16[512,256]{1,0:T(8,128)(2,1)S(1)}, u32[]{:S(2)}, u32[]{:S(2)}) %collective-permute-start.4) | collective-permute-done | bytes 262176 | tf_op jit(solution)/shard_map/ppermute | solution.py:51
  76.0 0.0 collective-permute-start.5
  76.0 15.2 %collective-permute-done.5 = bf16[512,256]{1,0:T(8,128)(2,1)S(1)} collective-permute-done((bf16[512,256]{1,0:T(8,128)(2,1)S(1)}, bf16[512,256]{1,0:T(8,128)(2,1)S(1)}, u32[]{:S(2)}, u32[]{:S(2)}) %collective-permute-start.5) | collective-permute-done | bytes 262176 | tf_op jit(solution)/shard_map/ppermute | solution.py:51
  91.1 0.0 collective-permute-start.6
  91.1 0.8 fusion.31
  92.0 8.3 %collective-permute-done.6 = bf16[512,256]{1,0:T(8,128)(2,1)S(1)} collective-permute-done((bf16[512,256]{1,0:T(8,128)(2,1)S(1)}, bf16[512,256]{1,0:T(8,128)(2,1)S(1)}, u32[]{:S(2)}, u32[]{:S(2)}) %collective-permute-start.6) | collective-permute-done | bytes 262176 | tf_op jit(solution)/shard_map/ppermute | solution.py:51
  100.2 0.7 constant_dynamic-update-slice_fusion.15
  101.0 0.8 constant_dynamic-update-slice_fusion.14
  101.7 0.8 constant_dynamic-update-slice_fusion.13
  102.5 0.8 constant_dynamic-update-slice_fusion.12
  103.3 0.8 constant_dynamic-update-slice_fusion.11
  104.1 0.7 constant_dynamic-update-slice_fusion.10
  104.8 0.7 constant_dynamic-update-slice_fusion.9
  105.5 0.7 constant_dynamic-update-slice_fusion.8
  106.3 0.7 constant_dynamic-update-slice_fusion.7
  107.0 0.8 constant_dynamic-update-slice_fusion.6
  107.7 0.8 constant_dynamic-update-slice_fusion.5
  108.5 0.7 constant_dynamic-update-slice_fusion.4
  109.2 0.8 constant_dynamic-update-slice_fusion.3
  110.0 0.7 constant_dynamic-update-slice_fusion.2
  110.7 0.7 constant_dynamic-update-slice_fusion.1
  111.5 0.8 constant_dynamic-update-slice_fusion
  112.2 2.7 fusion.8
  114.9 23.5 %all-gather.12.cloned.1.call-done = bf16[2048,512]{1,0:T(8,128)(2,1)} async-done(((bf16[256,512]{1,0:T(8,128)(2,1)}), bf16[2048,512]{1,0:T(8,128)(2,1)}) %all-gather.12.cloned.1.call-update) | async-done | bytes 2097168 | tf_op jit(solution)/shard_map/all_gather | solution.py:33
  138.5 2.6 fusion.7
  141.1 47.0 %all-gather.10.cloned.1.call-done = bf16[2048,512]{1,0:T(8,128)(2,1)} async-done(((bf16[256,512]{1,0:T(8,128)(2,1)}), bf16[2048,512]{1,0:T(8,128)(2,1)}) %all-gather.10.cloned.1.call-update) | async-done | bytes 2097168 | tf_op jit(solution)/shard_map/all_gather | solution.py:32
  188.1 4.6 convolution_convert_fusion.1
  192.7 0.0 reduce-scatter.3.cloned.1.call-update
  192.8 0.0 all-gather.16.cloned.1.call-start
  192.8 7.0 reduce-scatter.3.cloned.1.call-done
  199.8 1.3 fusion.13
  201.1 2.0 fusion.15
  203.2 0.0 all-gather.16.cloned.1.call-update
  203.2 0.0 all-gather.18.cloned.1.call-start
  203.3 0.7 all-gather.18.cloned.1.call-update
  204.0 0.0 all-gather.20.cloned.1.call-start
  204.0 0.7 all-gather.20.cloned.1.call-update
  204.7 0.0 reduce-scatter.5.cloned.1.call-start
  204.8 8.9 %all-gather.16.cloned.1.call-done = bf16[256,2048]{1,0:T(8,128)(2,1)} async-done(((bf16[128,2048]{1,0:T(8,128)(2,1)}), bf16[256,2048]{1,0:T(8,128)(2,1)}) %all-gather.16.cloned.1.call-update) | async-done | bytes 1048592 | tf_op jit(solution)/shard_map/all_gather | solution.py:64
  213.6 230.6 %all-gather.18.cloned.1.call-done = bf16[2048,4096]{1,0:T(8,128)(2,1)} async-done(((bf16[256,4096]{1,0:T(8,128)(2,1)}), bf16[2048,4096]{1,0:T(8,128)(2,1)}) %all-gather.18.cloned.1.call-update) | async-done | bytes 16777232 | tf_op jit(solution)/shard_map/all_gather | solution.py:65
  444.2 227.6 %all-gather.20.cloned.1.call-done = bf16[4096,2048]{1,0:T(8,128)(2,1)} async-done(((bf16[4096,256]{1,0:T(8,128)(2,1)}), bf16[4096,2048]{1,0:T(8,128)(2,1)}) %all-gather.20.cloned.1.call-update) | async-done | bytes 16777232 | tf_op jit(solution)/shard_map/all_gather | solution.py:68
  671.8 16.5 %convolution_convert_fusion = bf16[256,2048]{1,0:T(8,128)(2,1)} fusion(bf16[4096,2048]{1,0:T(8,128)(2,1)} %all-gather.20.cloned.1.call-done, bf16[256,2048]{1,0:T(8,128)(2,1)} %all-gather.16.cloned.1.call-done, bf16[2048,4096]{1,0:T(8,128)(2,1)} %all-gather.18.cloned.1.call-done), kind=kOutput, calls=%fused_computation.3 | convolution fusion | flops 8593604608 | bytes 35651584 | tf_op jit(solution)/shard_map/dot_general | solution.py:71
  688.3 0.0 reduce-scatter.5.cloned.1.call-update
  688.3 6.7 reduce-scatter.5.cloned.1.call-done
  695.0 2.1 fusion.16
  (15 shorter events, 0.0 us)
Async XLA Ops:
  6.5 99.0 %copy-start.2 = (bf16[512,256]{1,0:T(8,128)(2,1)S(1)}, bf16[512,256]{1,0:T(8,128)(2,1)}, u32[]{:S(2)}) copy-start(bf16[512,256]{1,0:T(8,128)(2,1)} %param.16) | copy-start | bytes 786436
  6.5 105.7 %all-gather.8.cloned.1.call-start = ((), (), s32[]{:S(2)}) async-start(), calls=%async_computation.2 | async-start | bytes 1572864 | tf_op jit(solution)/shard_map/all_gather | solution.py:28
  9.9 102.4 %all-gather.14.cloned.1.call-start = ((), (), s32[]{:S(2)}) async-start(), calls=%async_computation.5 | async-start | bytes 2359296 | tf_op jit(solution)/shard_map/all_gather | solution.py:31
  10.6 127.8 %all-gather.12.cloned.1.call-start = ((), (), s32[]{:S(2)}) async-start(), calls=%async_computation.4 | async-start | bytes 2359296 | tf_op jit(solution)/shard_map/all_gather | solution.py:33
  11.4 176.7 %all-gather.10.cloned.1.call-start = ((), (), s32[]{:S(2)}) async-start(), calls=%async_computation.3 | async-start | bytes 2359296 | tf_op jit(solution)/shard_map/all_gather | solution.py:32
  11.4 12.6 %collective-permute-start = (bf16[512,256]{1,0:T(8,128)(2,1)}, bf16[512,256]{1,0:T(8,128)(2,1)S(1)}, u32[]{:S(2)}, u32[]{:S(2)}) collective-permute-start(bf16[512,256]{1,0:T(8,128)(2,1)} %param.16), channel_id=1, source_target_pairs={{0,2},{2,4},{4,6},{6,8},{8,10},{10,12},{12,14},{14,0},{1,3},{3,5},... | collective-permute-start | bytes 786440 | tf_op jit(solution)/shard_map/ppermute | solution.py:51
  24.0 10.2 %collective-permute-start.1 = (bf16[512,256]{1,0:T(8,128)(2,1)S(1)}, bf16[512,256]{1,0:T(8,128)(2,1)S(1)}, u32[]{:S(2)}, u32[]{:S(2)}) collective-permute-start(bf16[512,256]{1,0:T(8,128)(2,1)S(1)} %collective-permute-done), channel_id=1, source_target_pairs={{0,2},{2,4},{4,6},{6,8},{8,10},{10,12},{12,14},{14,0},{1,3},{3,5},... | collective-permute-start | bytes 786440 | tf_op jit(solution)/shard_map/ppermute | solution.py:51
  34.2 16.1 %collective-permute-start.2 = (bf16[512,256]{1,0:T(8,128)(2,1)S(1)}, bf16[512,256]{1,0:T(8,128)(2,1)S(1)}, u32[]{:S(2)}, u32[]{:S(2)}) collective-permute-start(bf16[512,256]{1,0:T(8,128)(2,1)S(1)} %collective-permute-done.1), channel_id=1, source_target_pairs={{0,2},{2,4},{4,6},{6,8},{8,10},{10,12},{12,14},{14,0},{1,3},{3,5},... | collective-permute-start | bytes 786440 | tf_op jit(solution)/shard_map/ppermute | solution.py:51
  34.2 165.6 %reduce-scatter.3.cloned.1.call-start = ((), (), s32[]{:S(2)}) async-start(), calls=%async_computation.6 | async-start | bytes 1572864 | tf_op jit(solution)/shard_map/reduce_scatter | solution.py:56
  50.3 9.1 %collective-permute-start.3 = (bf16[512,256]{1,0:T(8,128)(2,1)S(1)}, bf16[512,256]{1,0:T(8,128)(2,1)S(1)}, u32[]{:S(2)}, u32[]{:S(2)}) collective-permute-start(bf16[512,256]{1,0:T(8,128)(2,1)S(1)} %collective-permute-done.2), channel_id=1, source_target_pairs={{0,2},{2,4},{4,6},{6,8},{8,10},{10,12},{12,14},{14,0},{1,3},{3,5},... | collective-permute-start | bytes 786440 | tf_op jit(solution)/shard_map/ppermute | solution.py:51
  59.3 16.6 %collective-permute-start.4 = (bf16[512,256]{1,0:T(8,128)(2,1)S(1)}, bf16[512,256]{1,0:T(8,128)(2,1)S(1)}, u32[]{:S(2)}, u32[]{:S(2)}) collective-permute-start(bf16[512,256]{1,0:T(8,128)(2,1)S(1)} %collective-permute-done.3), channel_id=1, source_target_pairs={{0,2},{2,4},{4,6},{6,8},{8,10},{10,12},{12,14},{14,0},{1,3},{3,5},... | collective-permute-start | bytes 786440 | tf_op jit(solution)/shard_map/ppermute | solution.py:51
  76.0 15.2 %collective-permute-start.5 = (bf16[512,256]{1,0:T(8,128)(2,1)S(1)}, bf16[512,256]{1,0:T(8,128)(2,1)S(1)}, u32[]{:S(2)}, u32[]{:S(2)}) collective-permute-start(bf16[512,256]{1,0:T(8,128)(2,1)S(1)} %collective-permute-done.4), channel_id=1, source_target_pairs={{0,2},{2,4},{4,6},{6,8},{8,10},{10,12},{12,14},{14,0},{1,3},{3,5},... | collective-permute-start | bytes 786440 | tf_op jit(solution)/shard_map/ppermute | solution.py:51
  91.1 9.1 %collective-permute-start.6 = (bf16[512,256]{1,0:T(8,128)(2,1)S(1)}, bf16[512,256]{1,0:T(8,128)(2,1)S(1)}, u32[]{:S(2)}, u32[]{:S(2)}) collective-permute-start(bf16[512,256]{1,0:T(8,128)(2,1)S(1)} %collective-permute-done.5), channel_id=1, source_target_pairs={{0,2},{2,4},{4,6},{6,8},{8,10},{10,12},{12,14},{14,0},{1,3},{3,5},... | collective-permute-start | bytes 786440 | tf_op jit(solution)/shard_map/ppermute | solution.py:51
  112.2 75.9 %copy-start.3 = (bf16[256,2048]{1,0:T(8,128)(2,1)S(1)}, bf16[256,2048]{1,0:T(8,128)(2,1)}, u32[]{:S(2)}) copy-start(bf16[256,2048]{1,0:T(8,128)(2,1)} %all-gather.8.cloned.1.call-done) | copy-start | bytes 3145732
  188.1 11.7 %copy-start = (bf16[128,2048]{1,0:T(8,128)(2,1)S(1)}, bf16[128,2048]{1,0:T(8,128)(2,1)}, u32[]{:S(2)}) copy-start(bf16[128,2048]{1,0:T(8,128)(2,1)} %param.10) | copy-start | bytes 1572868
  188.1 13.0 %copy-start.4 = (f32[2048]{0:T(1024)S(1)}, f32[2048]{0:T(1024)}, u32[]{:S(2)}) copy-start(f32[2048]{0:T(1024)} %param.17) | copy-start | bytes 24580
  192.8 20.9 %all-gather.16.cloned.1.call-start = ((), (), s32[]{:S(2)}) async-start(), calls=%async_computation.7 | async-start | bytes 1572864 | tf_op jit(solution)/shard_map/all_gather | solution.py:64
  203.2 241.0 %all-gather.18.cloned.1.call-start = ((), (), s32[]{:S(2)}) async-start(), calls=%async_computation.8 | async-start | bytes 18874368 | tf_op jit(solution)/shard_map/all_gather | solution.py:65
  204.0 467.8 %all-gather.20.cloned.1.call-start = ((), (), s32[]{:S(2)}) async-start(), calls=%async_computation.9 | async-start | bytes 18874368 | tf_op jit(solution)/shard_map/all_gather | solution.py:68
  204.7 490.3 %copy-start.1 = (bf16[128,2048]{1,0:T(8,128)(2,1)S(1)}, bf16[128,2048]{1,0:T(8,128)(2,1)}, u32[]{:S(2)}) copy-start(bf16[128,2048]{1,0:T(8,128)(2,1)} %reduce-scatter.3.cloned.1.call-done) | copy-start | bytes 1572868
  204.7 490.3 %reduce-scatter.5.cloned.1.call-start = ((), (), s32[]{:S(2)}) async-start(), calls=%async_computation.10 | async-start | bytes 1572864 | tf_op jit(solution)/shard_map/reduce_scatter | solution.py:70
Sparse Core Ops, SparseCore 0:
  10.0 11.7 all-gather.7
  23.9 61.6 all-gather.13
  87.8 50.6 all-gather.11
  140.4 47.6 all-gather.9
  192.9 6.8 reduce-scatter.2
  203.3 10.2 all-gather.15
  215.8 228.4 all-gather.17
  446.3 225.4 all-gather.19
  688.4 6.5 reduce-scatter.4
